TPU v7x, 32 devices: a whole 2x2x4 slice. The times are simulated.
32 devices in a mesh: ep: 8 (over z, x), tp: 4 (over y, core).
Axes of the slice: x: 2, y: 2, z: 4, core: 2. Of those that a mesh axis runs over, the one named last changes fastest.
Arguments:
- tokens: bfloat16 [192, 3072], P('ep'), may hold values from -6 to 6
- norm_gain: float32 [3072], replicated, may hold values from 0.1 to 1.9
- routing: int32 [192, 4], P('ep'), may hold values from 0 to 7, all different within a row; in each aligned block of 24 rows (0 to 23, 24 to 47, ...) at most 13 rows name the same one
- route_weight: float32 [192, 4], P('ep'), may hold values from 0.05 to 1
- w_gate: bfloat16 [8, 3072, 3072], P('ep', None, 'tp'), may hold values from -0.3125 to 0.3125
- w_up: bfloat16 [8, 3072, 3072], P('ep', None, 'tp'), may hold values from -0.3125 to 0.3125
- w_down: bfloat16 [8, 3072, 3072], P('ep', 'tp'), may hold values from -0.01953125 to 0.01953125
Outputs:
- mixed: bfloat16 [192, 3072], P('ep', 'tp')
Inputs may be any that keep to these rules, and one draw needn't show every extreme that they name: `routing`: each row names 4 different experts. Within the rows of one device (aligned blocks of 24 rows) no expert is named by more than 13 rows, a bound that some block reaches.
All inputs are finite; a program needn't handle non-finite values.
Results may differ from a plain program's by a relative error of at most 0.019.
Values may be sent and summed in bfloat16 or wider, within the bound.
No kernel may reach another device: no remote copies, remote signals or barrier semaphores. Data moves between devices by JAX's collectives and lax.ppermute only.
A program may use at most 64 MiB of HBM per device.

v0:
```python
import jax
import jax.numpy as jnp
from jax import lax
from jax.sharding import PartitionSpec as P

NORM_EPS = 1e-06
CLAMP_LIMIT = 7.0
SIGMOID_SCALE = 1.702


def slot_index(route_rows, expert_total, capacity):
    flat_ids = route_rows.reshape(-1)
    one_hot = (flat_ids[:, None] == jnp.arange(expert_total, dtype=jnp.int32)[None, :]).astype(
        jnp.int32
    )
    before = jnp.cumsum(one_hot, axis=0) - one_hot
    ranked = jnp.sum(before * one_hot, axis=1)
    return flat_ids * capacity + ranked


def local(tokens, norm_gain, routing, route_weight, w_gate, w_up, w_down):
    tok_count = tokens.shape[0]
    width = tokens.shape[1]
    top_count = routing.shape[1]
    expert_total = lax.axis_size("ep") * w_gate.shape[0]
    capacity = max(2, tok_count * top_count // expert_total + 1)
    slice_width = width // lax.axis_size("tp")
    values = tokens.astype(jnp.float32)
    scaled = values * lax.rsqrt(jnp.mean(values * values, axis=-1, keepdims=True) + NORM_EPS)
    normal = (scaled * norm_gain).astype(jnp.bfloat16)
    dest = slot_index(routing, expert_total, capacity)
    slot_ids = jnp.arange(expert_total * capacity, dtype=jnp.int32)
    select = jnp.sum(dest.reshape(1, tok_count, top_count) == slot_ids[:, None, None], axis=2)
    sending = jnp.dot(
        select.astype(jnp.bfloat16), normal, preferred_element_type=jnp.float32
    ).astype(jnp.bfloat16)
    gate_mat = w_gate[0]
    up_mat = w_up[0]
    down_mat = w_down[0]
    own_share = lax.dynamic_slice_in_dim(
        sending, lax.axis_index("tp") * slice_width, slice_width, 1
    )
    arrived = lax.all_to_all(own_share, "ep", split_axis=0, concat_axis=0, tiled=True)
    pieces = lax.all_gather(arrived, "tp", axis=1, tiled=True)
    gate_pre = jnp.dot(pieces, gate_mat, preferred_element_type=jnp.float32)
    up_pre = jnp.dot(pieces, up_mat, preferred_element_type=jnp.float32)
    gated = jnp.minimum(gate_pre, CLAMP_LIMIT)
    upper = jnp.clip(up_pre, -CLAMP_LIMIT, CLAMP_LIMIT)
    hidden = ((upper + 1.0) * gated * jax.nn.sigmoid(SIGMOID_SCALE * gated)).astype(jnp.bfloat16)
    summed = lax.psum_scatter(
        lax.dot_general(
            down_mat, hidden, (((0,), (1,)), ((), ())), preferred_element_type=jnp.float32
        ).astype(jnp.bfloat16),
        "tp",
        scatter_dimension=0,
        tiled=True,
    )
    back = lax.all_to_all(summed, "ep", split_axis=1, concat_axis=1, tiled=True)
    picked = back[:, dest].reshape(slice_width, tok_count, top_count)
    mixed = jnp.sum(picked.astype(jnp.float32) * route_weight[None, :, :], axis=2)
    return mixed.T.astype(jnp.bfloat16)


def solution(mesh):
    placed = (
        P("ep", None),
        P(),
        P("ep", None),
        P("ep", None),
        P("ep", None, "tp"),
        P("ep", None, "tp"),
        P("ep", "tp", None),
    )
    return jax.shard_map(
        local, mesh=mesh, in_specs=placed, out_specs=P("ep", "tp"), check_vma=False
    )
```

profile of v0, /device:TPU:0, one launch (start us, length us, event | category | flops | bytes accessed | tf_op | source)
XLA Modules:
  0.0 87.3 jit_solution(828306079801427838)
XLA Ops:
  6.5 0.8 copy.14
  7.3 0.1 eq.28
  7.4 0.1 fusion.48
  7.5 0.1 reduce_window_sum.11
  7.6 0.2 select_reduce_fusion
  7.8 0.1 reduce_sum.41
  7.9 0.1 copy.16
  8.0 0.1 convert_reduce_fusion
  8.1 1.0 %fusion.37 = f32[24]{0:T(128)S(1)} fusion(bf16[24,3072]{1,0:T(8,128)(2,1)} %param.7), kind=kLoop, calls=%fused_computation.23 | loop fusion | flops 221160 | bytes 147552 | tf_op jit(solution)/shard_map/reduce_sum | solution.py:29
  9.2 1.3 %fusion.44 = bf16[104,3072]{1,0:T(8,128)(2,1)S(1)} fusion(bf16[24,3072]{1,0:T(8,128)(2,1)} %param.7, f32[3072]{0:T(1024)} %param.8, f32[24]{0:T(128)S(1)} %add_rsqrt_fusion, s32[104,24]{0,1:T(8,128)S(1)} %convert_reduce_fusion), kind=kOutput, calls=%fused_computation.32 | convolution fusion | flops 15632832 | bytes 808800 | tf_op jit(solution)/shard_map/dot_general | solution.py:34
  10.6 15.0 %all_to_all.24 = bf16[8,13,768]{2,1,0:T(8,128)(2,1)S(1)} all-to-all(bf16[8,13,768]{2,1,0:T(8,128)(2,1)S(1)} %all_to_all.16), channel_id=1, replica_groups=mesh['ep'=8,'tp'=4] {'ep'}, dimensions={0} | all-to-all | bytes 319488 | tf_op jit(solution)/shard_map/all_to_all | solution.py:43
  25.6 0.1 all_to_all.18
  25.7 7.8 %all_gather.3 = bf16[104,3072]{1,0:T(8,128)(2,1)S(1)} all-gather(bf16[104,768]{1,0:T(8,128)(2,1)S(1)} %all_to_all.18), channel_id=1, replica_groups=mesh['ep'=8,'tp'=4] {'tp'}, dimensions={1}, use_global_device_ids=true | all-gather | bytes 798720 | tf_op jit(solution)/shard_map/all_gather | solution.py:44
  33.5 3.2 %fusion.12 = f32[104,768]{1,0:T(8,128)S(1)} fusion(bf16[104,3072]{1,0:T(8,128)(2,1)S(1)} %all_gather.3, bf16[1,3072,768]{2,1,0:T(8,128)(2,1)} %param.11), kind=kOutput, calls=%fused_computation.9 | convolution fusion | flops 490813440 | bytes 5677056 | tf_op jit(solution)/shard_map/dot_general | solution.py:45
  36.7 6.5 %fusion.9 = bf16[3072,104]{0,1:T(8,128)(2,1)} fusion(bf16[1,768,3072]{2,1,0:T(8,128)(2,1)} %param.13, f32[104,768]{1,0:T(8,128)S(1)} %fusion.12, bf16[104,3072]{1,0:T(8,128)(2,1)S(1)} %all_gather.3, bf16[1,3072,768]{2,1,0:T(8,128)(2,1)} %param.12), kind=kOutput, calls=%fused_computation.8 | convolution fusion | flops 982505472 | bytes 11034624 | tf_op jit(solution)/shard_map/dot_general | solution.py:51
  43.2 0.1 mul.76
  43.4 0.1 copy.17
  43.4 20.2 %reduce-scatter.2.cloned.1.call-done = bf16[768,104]{0,1:T(8,128)(2,1)} async-done(((bf16[3072,104]{0,1:T(8,128)(2,1)}), bf16[768,104]{0,1:T(8,128)(2,1)}) %reduce-scatter.2.cloned.1.call-update) | async-done | bytes 159760 | tf_op jit(solution)/shard_map/reduce_scatter | solution.py:50
  63.7 1.6 %all_to_all.19 = bf16[768,8,13]{0,2,1:T(8,128)(2,1)} reshape(bf16[768,104]{0,1:T(8,128)(2,1)} %reduce-scatter.2.cloned.1.call-done) | data formatting | bytes 319488 | tf_op jit(solution)/shard_map/all_to_all | solution.py:58
  65.3 5.5 %all-to-all-start.1 = ((bf16[768,8,13]{0,2,1:T(8,128)(2,1)}), bf16[768,8,13]{0,2,1:T(8,128)(2,1)S(1)}, u32[]{:S(2)}, u32[]{:S(2)}) async-start(bf16[768,8,13]{0,2,1:T(8,128)(2,1)} %all_to_all.19), calls=%async_computation.2 | async-start | bytes 393216 | tf_op jit(solution)/shard_map/all_to_all | solution.py:58
  70.8 7.8 %all-to-all-done.1 = bf16[768,8,13]{0,2,1:T(8,128)(2,1)S(1)} async-done(((bf16[768,8,13]{0,2,1:T(8,128)(2,1)}), bf16[768,8,13]{0,2,1:T(8,128)(2,1)S(1)}, u32[]{:S(2)}, u32[]{:S(2)}) %all-to-all-start.1) | async-done | bytes 159776 | tf_op jit(solution)/shard_map/all_to_all | solution.py:58
  78.7 0.8 gather_fusion
  79.5 0.1 reshape.54
  79.6 0.9 multiply_reduce_fusion
  (12 shorter events, 0.2 us)
Async XLA Ops:
  6.5 57.1 %reduce-scatter.2.cloned.1.call-start = ((), (), s32[]{:S(2)}) async-start(), calls=%async_computation.3 | async-start | bytes 798720 | tf_op jit(solution)/shard_map/reduce_scatter | solution.py:50
  36.7 6.7 %copy-start = (f32[24,4]{0,1:T(4,128)S(1)}, f32[24,4]{0,1:T(4,128)}, u32[]{:S(2)}) copy-start(f32[24,4]{0,1:T(4,128)} %param.10) | copy-start | bytes 1156
  65.3 13.3 %all-to-all-start.1 = ((bf16[768,8,13]{0,2,1:T(8,128)(2,1)}), bf16[768,8,13]{0,2,1:T(8,128)(2,1)S(1)}, u32[]{:S(2)}, u32[]{:S(2)}) async-start(bf16[768,8,13]{0,2,1:T(8,128)(2,1)} %all_to_all.19), calls=%async_computation.2 | async-start | bytes 393216 | tf_op jit(solution)/shard_map/all_to_all | solution.py:58
Sparse Core Ops, SparseCore 0:
  43.4 20.2 reduce-scatter.1
where the time goes:
time: 87.7 us; the launch traced here: 87.3 us
  waiting for transfers between devices  28 us (32%)
  blocking collectives  22.9 us (26%)
  between operations  13.5 us (15%)
  matrix products  11 us (13%)
  starting transfers between devices  5.5 us (6%)
  local copies, waits for them, and re-layouts  3.96 us (5%)
  other arithmetic  2.44 us (3%)
    reduce_scatter x1, waiting for transfers between devices, local(): lax.psum_scatter(lax.dot_general(down_mat, hidden, (((0,), (1,)), ((), ()...  20.2 us
    all_to_all x1, blocking collectives, local(): lax.all_to_all(own_share, 'ep', split_axis=0, concat_axis=0, tiled=True)  15 us
    all_gather x1, blocking collectives, local(): pieces = lax.all_gather(arrived, 'tp', axis=1, tiled=True)  7.82 us
    all_to_all x1, waiting for transfers between devices, local(): back = lax.all_to_all(summed, 'ep', split_axis=1, concat_axis=1, tiled=True)  7.77 us
    dot_general x1, matrix products, local(): lax.dot_general(down_mat, hidden, (((0,), (1,)), ((), ())), preferred_ele...  6.54 us
    all_to_all x1, starting transfers between devices, local(): back = lax.all_to_all(summed, 'ep', split_axis=1, concat_axis=1, tiled=True)  5.5 us
    dot_general x1, matrix products, local(): gate_pre = jnp.dot(pieces, gate_mat, preferred_element_type=jnp.float32)  3.18 us
  transfers between devices with their start and end apart: 2, of which 2 were waited for; matrix products, arithmetic and copies ran while one was open for 0% of the time, Pallas kernels for 0%

commit v1 on v0

--- a/solution.py
+++ b/solution.py
@@ -1,3 +1,4 @@
+import functools
 import jax
 import jax.numpy as jnp
 from jax import lax
@@ -6,6 +7,14 @@
 NORM_EPS = 1e-06
 CLAMP_LIMIT = 7.0
 SIGMOID_SCALE = 1.702
+
+
+def spread_waves(a0, a_name, along_dim):
+    after = jnp.concatenate(lax.all_gather(a0, a_name), axis=along_dim)
+    return after
+
+
+panel_pass = functools.partial(spread_waves, a_name="tp", along_dim=1)
 
 
 def slot_index(route_rows, expert_total, capacity):
@@ -41,7 +50,7 @@
         sending, lax.axis_index("tp") * slice_width, slice_width, 1
     )
     arrived = lax.all_to_all(own_share, "ep", split_axis=0, concat_axis=0, tiled=True)
-    pieces = lax.all_gather(arrived, "tp", axis=1, tiled=True)
+    pieces = panel_pass(arrived)
     gate_pre = jnp.dot(pieces, gate_mat, preferred_element_type=jnp.float32)
     up_pre = jnp.dot(pieces, up_mat, preferred_element_type=jnp.float32)
     gated = jnp.minimum(gate_pre, CLAMP_LIMIT)

time: 87.7 us -> 87.7 us (level)
  no operation moved by 1% of the time
where the time goes in v1:
time: 87.7 us; the launch traced here: 87.4 us
  waiting for transfers between devices  28 us (32%)
  blocking collectives  22.9 us (26%)
  between operations  13.5 us (15%)
  matrix products  11 us (13%)
  starting transfers between devices  5.53 us (6%)
  local copies, waits for them, and re-layouts  4.02 us (5%)
  other arithmetic  2.44 us (3%)
    reduce_scatter x1, waiting for transfers between devices, local(): lax.psum_scatter(lax.dot_general(down_mat, hidden, (((0,), (1,)), ((), ()...  20.2 us
    all_to_all x1, blocking collectives, local(): lax.all_to_all(own_share, 'ep', split_axis=0, concat_axis=0, tiled=True)  15 us
    all_gather x1, blocking collectives, spread_waves(): after = jnp.concatenate(lax.all_gather(a0, a_name), axis=along_dim)  7.82 us
    all_to_all x1, waiting for transfers between devices, local(): back = lax.all_to_all(summed, 'ep', split_axis=1, concat_axis=1, tiled=True)  7.77 us
    dot_general x1, matrix products, local(): lax.dot_general(down_mat, hidden, (((0,), (1,)), ((), ())), preferred_ele...  6.54 us
    all_to_all x1, starting transfers between devices, local(): back = lax.all_to_all(summed, 'ep', split_axis=1, concat_axis=1, tiled=True)  5.52 us
    dot_general x1, matrix products, local(): gate_pre = jnp.dot(pieces, gate_mat, preferred_element_type=jnp.float32)  3.18 us
  transfers between devices with their start and end apart: 2, of which 2 were waited for; matrix products, arithmetic and copies ran while one was open for 0% of the time, Pallas kernels for 0%

profile of v1, /device:TPU:0, one launch (start us, length us, event | category | flops | bytes accessed | tf_op | source)
XLA Modules:
  0.0 87.4 jit_solution(16225843954624104547)
XLA Ops:
  6.5 0.8 copy.19
  7.3 0.1 eq.28
  7.4 0.1 fusion.48
  7.5 0.1 reduce_window_sum.11
  7.6 0.2 select_reduce_fusion
  7.8 0.1 reduce_sum.41
  7.9 0.1 copy.21
  8.0 0.1 convert_reduce_fusion
  8.1 1.0 %fusion.37 = f32[24]{0:T(128)S(1)} fusion(bf16[24,3072]{1,0:T(8,128)(2,1)} %param.7), kind=kLoop, calls=%fused_computation.23 | loop fusion | flops 221160 | bytes 147552 | tf_op jit(solution)/shard_map/reduce_sum | solution.py:38
  9.2 1.3 %fusion.44 = bf16[104,3072]{1,0:T(8,128)(2,1)S(1)} fusion(bf16[24,3072]{1,0:T(8,128)(2,1)} %param.7, f32[3072]{0:T(1024)} %param.8, f32[24]{0:T(128)S(1)} %add_rsqrt_fusion, s32[104,24]{0,1:T(8,128)S(1)} %convert_reduce_fusion), kind=kOutput, calls=%fused_computation.32 | convolution fusion | flops 15632832 | bytes 808800 | tf_op jit(solution)/shard_map/dot_general | solution.py:43
  10.6 15.0 %all_to_all.21 = bf16[8,13,768]{2,1,0:T(8,128)(2,1)S(1)} all-to-all(bf16[8,13,768]{2,1,0:T(8,128)(2,1)S(1)} %all_to_all.14), channel_id=1, replica_groups=mesh['ep'=8,'tp'=4] {'ep'}, dimensions={0} | all-to-all | bytes 319488 | tf_op jit(solution)/shard_map/all_to_all | solution.py:52
  25.6 0.1 all_gather.6
  25.7 7.8 %all_gather.7 = bf16[4,104,768]{2,1,0:T(8,128)(2,1)S(1)} all-gather(bf16[1,104,768]{2,1,0:T(8,128)(2,1)S(1)} %all_gather.6), channel_id=1, replica_groups=mesh['ep'=8,'tp'=4] {'tp'}, dimensions={0}, use_global_device_ids=true | all-gather | bytes 798720 | tf_op jit(solution)/shard_map/all_gather | solution.py:13
  33.6 3.2 %fusion.12 = f32[104,768]{1,0:T(8,128)S(1)} fusion(bf16[104,3072]{1,0:T(8,128)(2,1)S(1)} %bitcast.51, bf16[1,3072,768]{2,1,0:T(8,128)(2,1)} %param.11), kind=kOutput, calls=%fused_computation.9 | convolution fusion | flops 490813440 | bytes 5677056 | tf_op jit(solution)/shard_map/dot_general | solution.py:54
  36.7 6.5 %fusion.9 = bf16[3072,104]{0,1:T(8,128)(2,1)} fusion(bf16[1,768,3072]{2,1,0:T(8,128)(2,1)} %param.13, f32[104,768]{1,0:T(8,128)S(1)} %fusion.12, bf16[104,3072]{1,0:T(8,128)(2,1)S(1)} %bitcast.52, bf16[1,3072,768]{2,1,0:T(8,128)(2,1)} %param.12), kind=kOutput, calls=%fused_computation.8 | convolution fusion | flops 982505472 | bytes 11034624 | tf_op jit(solution)/shard_map/dot_general | solution.py:60
  43.3 0.1 mul.76
  43.4 0.1 copy.23
  43.5 20.2 %reduce-scatter.2.cloned.1.call-done = bf16[768,104]{0,1:T(8,128)(2,1)} async-done(((bf16[3072,104]{0,1:T(8,128)(2,1)}), bf16[768,104]{0,1:T(8,128)(2,1)}) %reduce-scatter.2.cloned.1.call-update) | async-done | bytes 159760 | tf_op jit(solution)/shard_map/reduce_scatter | solution.py:59
  63.7 1.6 %all_to_all.16 = bf16[768,8,13]{0,2,1:T(8,128)(2,1)} reshape(bf16[768,104]{0,1:T(8,128)(2,1)} %reduce-scatter.2.cloned.1.call-done) | data formatting | bytes 319488 | tf_op jit(solution)/shard_map/all_to_all | solution.py:67
  65.4 5.5 %all-to-all-start.1 = ((bf16[768,8,13]{0,2,1:T(8,128)(2,1)}), bf16[768,8,13]{0,2,1:T(8,128)(2,1)S(1)}, u32[]{:S(2)}, u32[]{:S(2)}) async-start(bf16[768,8,13]{0,2,1:T(8,128)(2,1)} %all_to_all.16), calls=%async_computation.2 | async-start | bytes 393216 | tf_op jit(solution)/shard_map/all_to_all | solution.py:67
  70.9 7.8 %all-to-all-done.1 = bf16[768,8,13]{0,2,1:T(8,128)(2,1)S(1)} async-done(((bf16[768,8,13]{0,2,1:T(8,128)(2,1)}), bf16[768,8,13]{0,2,1:T(8,128)(2,1)S(1)}, u32[]{:S(2)}, u32[]{:S(2)}) %all-to-all-start.1) | async-done | bytes 159776 | tf_op jit(solution)/shard_map/all_to_all | solution.py:67
  78.8 0.8 gather_fusion
  79.6 0.1 reshape.63
  79.7 0.9 multiply_reduce_fusion
  (13 shorter events, 0.3 us)
Async XLA Ops:
  6.5 57.2 %reduce-scatter.2.cloned.1.call-start = ((), (), s32[]{:S(2)}) async-start(), calls=%async_computation.3 | async-start | bytes 798720 | tf_op jit(solution)/shard_map/reduce_scatter | solution.py:59
  36.7 6.7 %copy-start = (f32[24,4]{0,1:T(4,128)S(1)}, f32[24,4]{0,1:T(4,128)}, u32[]{:S(2)}) copy-start(f32[24,4]{0,1:T(4,128)} %param.10) | copy-start | bytes 1156
  65.4 13.3 %all-to-all-start.1 = ((bf16[768,8,13]{0,2,1:T(8,128)(2,1)}), bf16[768,8,13]{0,2,1:T(8,128)(2,1)S(1)}, u32[]{:S(2)}, u32[]{:S(2)}) async-start(bf16[768,8,13]{0,2,1:T(8,128)(2,1)} %all_to_all.16), calls=%async_computation.2 | async-start | bytes 393216 | tf_op jit(solution)/shard_map/all_to_all | solution.py:67
Sparse Core Ops, SparseCore 0:
  43.4 20.2 reduce-scatter.1
